TPU v7x, 256 devices: a 4x2x16 block of a 4x16x16 slice. The times are simulated.
256 devices in a mesh: grp: 2 (over y), sp: 32 (over z, core), tp: 4 (over x).
Axes of the slice: x: 4, y: 2, z: 16, core: 2. Of those that a mesh axis runs over, the one named last changes fastest.
The devices are a block of a 4x16x16 slice.
Arguments:
- query_wide: bfloat16 [32768, 1024], P(('grp', 'sp'), 'tp'), parts along dimension 0, may hold values from -6 to 6
- key_wide: bfloat16 [32768, 1024], P(('grp', 'sp'), 'tp'), parts along dimension 0, may hold values from -6 to 6
- value_wide: bfloat16 [32768, 1024], P(('grp', 'sp'), 'tp'), parts along dimension 0, may hold values from -6 to 6
- decay_wide: float32 [32768, 8], P(('grp', 'sp'), 'tp'), parts along dimension 0, may hold values from -2 to 0, as said below
- query_narrow: bfloat16 [32768, 1024], P(('grp', 'sp'), 'tp'), parts along dimension 0, may hold values from -6 to 6
- key_narrow: bfloat16 [32768, 1024], P(('grp', 'sp'), 'tp'), parts along dimension 0, may hold values from -6 to 6
- value_narrow: bfloat16 [32768, 1024], P(('grp', 'sp'), 'tp'), parts along dimension 0, may hold values from -6 to 6
- decay_narrow: float32 [32768, 16], P(('grp', 'sp'), 'tp'), parts along dimension 0, may hold values from -2 to 0, as said below
- residual: bfloat16 [32768, 2048], P(('grp', 'sp', 'tp')), parts along dimension 0, may hold values from -6 to 6
- out_wide: bfloat16 [1024, 2048], P('tp'), may hold values from -0.125 to 0.125
- out_narrow: bfloat16 [1024, 2048], P('tp'), may hold values from -0.125 to 0.125
- norm_gain: float32 [2048], replicated, may hold values from 0.1 to 1.9
- routes: int32 [32768, 2], P(('grp', 'sp', 'tp')), parts along dimension 0, may hold values from 0 to 31, all different within a row; in each aligned block of 128 rows (0 to 127, 128 to 255, ...) at most 12 rows name the same one
- route_weights: float32 [32768, 2], P(('grp', 'sp', 'tp')), parts along dimension 0, may hold values from 0.1 to 1
- expert_gate: bfloat16 [32, 2048, 2048], P('sp', None, 'tp'), may hold values from -0.375 to 0.375
- expert_up: bfloat16 [32, 2048, 2048], P('sp', None, 'tp'), may hold values from -0.375 to 0.375
- expert_down: bfloat16 [32, 2048, 2048], P('sp', 'tp'), may hold values from -0.03125 to 0.03125
Outputs:
- layer_out: bfloat16 [32768, 2048], P(('grp', 'sp', 'tp')), parts along dimension 0
There are 2 independent parts, one for each index of `grp`. A program takes and returns all parts, laid end to end along the dimension named above; an argument that names none is the same for every part. Nothing has to cross between parts.
Inputs may be any that keep to these rules, and one draw needn't show every extreme that they name: `decay_wide`: every entry is negative. `decay_narrow`: every entry is negative. `routes`: each row names 2 different experts; on the rows of one device no expert is named more than 12 times, a bound that some block reaches.
All inputs are finite; a program needn't handle non-finite values.
Results may differ from a plain program's by a relative error of at most 0.018.
Values may be sent and summed in bfloat16 or wider, within the bound.
No kernel may reach another device: no remote copies, remote signals or barrier semaphores. Data moves between devices by JAX's collectives and lax.ppermute only.
A program may use at most 128 MiB of HBM per device.

v0:
```python
import jax
import jax.numpy as jnp
from jax import lax
from jax.sharding import Mesh
from jax.sharding import PartitionSpec as P

HEAD_WIDE = 128
HEAD_NARROW = 64
TOP_K = 2
SP = ("sp_0", "sp_1")
GRP_SP = ("grp", "sp_0", "sp_1")
GRP_SP_TP = ("grp", "sp_0", "sp_1", "tp")
norm_eps = 1e-05
clamp_limit = 7.0
swish_alpha = 1.702
rotary_base = 10000.0


def filled_with(value, identity):
    return jax.tree.map(
        lambda a, e: jnp.broadcast_to(jnp.asarray(e, a.dtype), a.shape), value, identity
    )


def prefix_by_axis(value, axes, combine, identity):
    before = start = filled_with(value, identity)
    total = value
    for axis in reversed(axes):
        length, mine = (lax.axis_size(axis), lax.axis_index(axis))
        pieces = jax.tree.map(
            lambda part, kind: lax.all_gather(part.astype(kind), axis),
            total,
            jax.tree.map(lambda a: jnp.bfloat16 if a.dtype == jnp.float32 else a.dtype, value),
        )
        inside, total = (start, start)
        for k in range(length):
            passed = k < mine
            total = combine(
                total, jax.tree.map(lambda part, own: part[k].astype(own.dtype), pieces, value)
            )
            inside = jax.tree.map(lambda new, old: jnp.where(passed, new, old), total, inside)
        before = combine(inside, before)
    return before


def cut_along(value, dim, length):
    lengths = value.shape
    pieces = value.reshape(*lengths[:dim], length, lengths[dim] // length, *lengths[dim + 1 :])
    return jnp.moveaxis(pieces, dim, 0)


def sent_and_summed(value, axis, dim):
    pieces = cut_along(value, dim, lax.axis_size(axis))
    arrived = lax.all_to_all(pieces, axis, split_axis=0, concat_axis=0, tiled=True)
    return arrived.astype(jnp.float32).sum(axis=0)


def laid_out(pieces, dim):
    pieces = jnp.moveaxis(pieces, 0, dim)
    lengths = pieces.shape
    return pieces.reshape(*lengths[:dim], lengths[dim] * lengths[dim + 1], *lengths[dim + 2 :])


def turned_blocks(pieces, axes, order):
    inside = pieces.shape[1:]
    filled = pieces.reshape(*(lax.axis_size(a) for a in axes), *inside)
    for k in order:
        filled = lax.all_to_all(filled, axes[k], k, k, tiled=True)
    return filled.reshape(-1, *inside)


def core_and_chips(value, groups, order, split_dim, concat_dim):
    length = lax.axis_size(groups[0]) * lax.axis_size(groups[1])
    pieces = cut_along(value, split_dim, length)
    return laid_out(turned_blocks(pieces, groups, order), concat_dim)


def rotate(values, positions):
    half_width = values.shape[-1] // 2
    inverse = rotary_base ** (-jnp.arange(half_width, dtype=jnp.float32) / half_width)
    angles = positions[:, None] * inverse[None, :]
    cosine = jnp.cos(angles)[:, None, :]
    sine_part = jnp.sin(angles)[:, None, :]
    lower_half = values[..., :half_width]
    upper_half = values[..., half_width:]
    return jnp.concatenate(
        [
            lower_half * cosine - upper_half * sine_part,
            lower_half * sine_part + upper_half * cosine,
        ],
        axis=-1,
    )


def group_norm(output_heads):
    center = jnp.mean(output_heads, axis=-1, keepdims=True)
    spread = jnp.mean(jnp.square(output_heads - center), axis=-1, keepdims=True)
    return (output_heads - center) * lax.rsqrt(spread + norm_eps)


def local_terms(query_in, key_in, value_in, log_decay, head_width, positions):
    length = query_in.shape[0]
    attention_group_count = query_in.shape[1] // head_width
    query_heads = query_in.astype(jnp.float32).reshape(length, attention_group_count, head_width)
    key_heads = key_in.astype(jnp.float32).reshape(length, attention_group_count, head_width)
    query_f = rotate(query_heads, positions).astype(jnp.bfloat16).astype(jnp.float32)
    key_f = (
        (rotate(key_heads, positions) * head_width ** (-0.5))
        .astype(jnp.bfloat16)
        .astype(jnp.float32)
    )
    value_f = value_in.reshape(length, attention_group_count, head_width).astype(jnp.float32)
    cumulative = jnp.cumsum(log_decay, axis=0)
    steps_in = jnp.arange(length, dtype=jnp.int32)
    causal = steps_in[:, None] >= steps_in[None, :]
    gaps = cumulative.T[:, :, None] - cumulative.T[:, None, :]
    decay_grid = jnp.exp(jnp.where(causal[None], gaps, -jnp.inf))
    scores = jnp.einsum("thd,shd->hts", query_f, key_f) * decay_grid
    inner_part = jnp.einsum("hts,she->the", scores, value_f)
    total_log = cumulative[-1]
    weighted = key_f * jnp.exp(total_log[None, :] - cumulative)[:, :, None]
    state_local = jnp.einsum("shd,she->hde", weighted, value_f)
    return (query_f, cumulative, inner_part, total_log, state_local)


def finish(parts, state_in):
    query_f, cumulative, inner_part = (parts[0], parts[1], parts[2])
    carried_part = jnp.exp(cumulative)[:, :, None] * jnp.einsum("thd,hde->the", query_f, state_in)
    normed_heads = group_norm(inner_part + carried_part)
    return normed_heads.reshape(normed_heads.shape[0], -1).astype(jnp.bfloat16)


def combine(earlier, later):
    return (
        earlier[0] + later[0],
        jnp.exp(later[0])[:, None, None] * earlier[1] + later[1],
        earlier[2] + later[2],
        jnp.exp(later[2])[:, None, None] * earlier[3] + later[3],
    )


def activate(gate_pre, up_pre):
    gate_clip = jnp.minimum(gate_pre, clamp_limit)
    up_clip = jnp.clip(up_pre, -clamp_limit, clamp_limit)
    return gate_clip * jax.nn.sigmoid(swish_alpha * gate_clip) * (up_clip + 1.0)


def body(
    query_wide,
    key_wide,
    value_wide,
    decay_wide,
    query_narrow,
    key_narrow,
    value_narrow,
    decay_narrow,
    residual,
    out_wide,
    out_narrow,
    norm_gain,
    routes,
    route_weights,
    expert_gate,
    expert_up,
    expert_down,
):
    length = query_wide.shape[0]
    tp_count = lax.axis_size("tp")
    experts = lax.axis_size(SP)
    model_width = residual.shape[1]
    positions = (lax.axis_index(SP) * length + jnp.arange(length, dtype=jnp.int32)).astype(
        jnp.float32
    )
    wide_parts = local_terms(query_wide, key_wide, value_wide, decay_wide, HEAD_WIDE, positions)
    narrow_parts = local_terms(
        query_narrow, key_narrow, value_narrow, decay_narrow, HEAD_NARROW, positions
    )
    local_states = (wide_parts[3], wide_parts[4], narrow_parts[3], narrow_parts[4])
    identity = tuple((jnp.zeros_like(member) for member in local_states))
    carried = prefix_by_axis(local_states, SP, combine, identity)
    mixed_wide = finish(wide_parts, carried[1])
    mixed_narrow = finish(narrow_parts, carried[3])
    rows_dev = length // tp_count
    attention = sent_and_summed(
        (
            jnp.dot(mixed_wide, out_wide, preferred_element_type=jnp.float32)
            + jnp.dot(mixed_narrow, out_narrow, preferred_element_type=jnp.float32)
        ).astype(jnp.bfloat16),
        "tp",
        0,
    )
    hidden_state = residual.astype(jnp.float32) + attention
    scale_row = lax.rsqrt(jnp.mean(hidden_state * hidden_state, axis=-1, keepdims=True) + norm_eps)
    normed = (hidden_state * scale_row * norm_gain).astype(jnp.bfloat16)
    capacity = max(2, 3 * rows_dev * TOP_K // (2 * experts))
    flat_expert = routes.reshape(-1)
    one_hot = (flat_expert[:, None] == jnp.arange(experts, dtype=jnp.int32)[None, :]).astype(
        jnp.int32
    )
    rank_in = jnp.sum((jnp.cumsum(one_hot, axis=0) - one_hot) * one_hot, axis=1)
    slot_index = flat_expert * capacity + rank_in
    source_row = jnp.arange(rows_dev * TOP_K, dtype=jnp.int32) // TOP_K
    slot_table = jnp.zeros((experts * capacity,), jnp.int32).at[slot_index].set(source_row + 1)
    padded = jnp.concatenate([jnp.zeros((1, model_width), jnp.bfloat16), normed], axis=0)
    send_slots = padded[slot_table].reshape(experts, capacity, model_width)
    gate_shard = expert_gate[0]
    up_shard = expert_up[0]
    down_shard = expert_down[0]
    gathered = lax.all_gather(
        core_and_chips(send_slots, ("sp_0", "sp_1"), (1, 0), 0, 0), "tp", axis=0, tiled=True
    )
    flat_rows = gathered.reshape(-1, model_width)
    gate_pre = jnp.dot(flat_rows, gate_shard, preferred_element_type=jnp.float32)
    up_pre = jnp.dot(flat_rows, up_shard, preferred_element_type=jnp.float32)
    hidden = activate(gate_pre, up_pre).astype(jnp.bfloat16)
    partial_value = jnp.dot(hidden, down_shard, preferred_element_type=jnp.float32)
    partial_value = partial_value.reshape(gathered.shape[0], gathered.shape[1], model_width)
    summed = sent_and_summed(
        partial_value.reshape(tp_count, experts, capacity, model_width).astype(jnp.bfloat16),
        "tp",
        0,
    )
    expert_output = summed.reshape(experts, capacity, model_width).astype(jnp.bfloat16)
    returned = lax.all_to_all(expert_output, SP, split_axis=0, concat_axis=0, tiled=True)
    picked = returned.reshape(experts * capacity, model_width)[slot_index].astype(jnp.float32)
    routed = jnp.sum(
        (picked * route_weights.reshape(-1)[:, None]).reshape(rows_dev, TOP_K, model_width), axis=1
    )
    return (hidden_state + routed).astype(jnp.bfloat16)


def solution(mesh):
    torus = Mesh(
        mesh.devices.reshape(mesh.shape["grp"], 16, 2, mesh.shape["tp"]),
        ("grp", "sp_0", "sp_1", "tp"),
    )
    in_specs = (
        P(GRP_SP, "tp"),
        P(GRP_SP, "tp"),
        P(GRP_SP, "tp"),
        P(GRP_SP, "tp"),
        P(GRP_SP, "tp"),
        P(GRP_SP, "tp"),
        P(GRP_SP, "tp"),
        P(GRP_SP, "tp"),
        P(GRP_SP_TP, None),
        P("tp", None),
        P("tp", None),
        P(),
        P(GRP_SP_TP, None),
        P(GRP_SP_TP, None),
        P(SP, None, "tp"),
        P(SP, None, "tp"),
        P(SP, "tp", None),
    )
    out_specs = P(GRP_SP_TP, None)
    return jax.shard_map(body, mesh=torus, in_specs=in_specs, out_specs=out_specs, check_vma=False)
```

profile of v0, /device:TPU:33, one launch (start us, length us, event | category | flops | bytes accessed | tf_op | source)
XLA Modules:
  0.0 619.4 jit_solution(2552972941295234430)
XLA Ops:
  19.9 2.4 subtract_convert_fusion
  23.0 22.0 %all-gather = bf16[4,128,128]{2,1,0:T(8,128)(2,1)S(1)} all-gather(bf16[2,128,128]{2,1,0:T(8,128)(2,1)S(1)} %convolution_convert_fusion.1), channel_id=2, replica_groups=mesh['grp'=2,'sp_0'=16,'sp_1'=2,'tp'=4] {'sp_1'}, dimensions={0}, use_global_device_ids=true | all-gather | bytes 196608 | tf_op jit(solution)/shard_map/all_gather | solution.py:31
  60.3 32.4 %all_gather.48 = bf16[16,4,64,64]{3,2,1,0:T(8,128)(2,1)S(1)} all-gather(bf16[1,4,64,64]{3,2,1,0:T(8,128)(2,1)S(1)} %fusion.70), channel_id=1, replica_groups=mesh['grp'=2,'sp_0'=16,'sp_1'=2,'tp'=4] {'sp_0'}, dimensions={0}, use_global_device_ids=true | all-gather | bytes 557056 | tf_op jit(solution)/shard_map/all_gather | solution.py:31
  92.8 21.5 %all-gather.5 = bf16[16,1,4]{2,1,0:T(2,128)(2,1)S(1)} all-gather(bf16[1,1,4]{2,1,0:T(2,128)(2,1)S(1)} %get-tuple-element.65), channel_id=1, replica_groups=mesh['grp'=2,'sp_0'=16,'sp_1'=2,'tp'=4] {'sp_0'}, dimensions={0}, use_global_device_ids=true | all-gather | bytes 136 | tf_op jit(solution)/shard_map/all_gather | solution.py:31
  115.0 19.9 %all-gather.3 = bf16[16,1,2]{2,1,0:T(2,128)(2,1)S(1)} all-gather(bf16[1,1,2]{2,1,0:T(2,128)(2,1)} %get-tuple-element.68), channel_id=1, replica_groups=mesh['grp'=2,'sp_0'=16,'sp_1'=2,'tp'=4] {'sp_0'}, dimensions={0}, use_global_device_ids=true | all-gather | bytes 68 | tf_op jit(solution)/shard_map/all_gather | solution.py:31
  136.3 4.1 fusion.31
  142.6 3.1 fusion.34
  145.7 2.5 fusion.326
  152.4 4.7 all-to-all-start
  160.2 12.2 %all-to-all-done = bf16[4,128,2048]{2,1,0:T(8,128)(2,1)} async-done(((bf16[4,128,2048]{2,1,0:T(8,128)(2,1)}), bf16[4,128,2048]{2,1,0:T(8,128)(2,1)}, u32[]{:S(2)}, u32[]{:S(2)}) %all-to-all-start) | async-done | bytes 2097184 | tf_op jit(solution)/shard_map/all_to_all | solution.py:54
  175.9 3.1 gather_fusion
  179.0 3.6 reshape_reshape_reshape.3
  182.6 2.5 copy.204
  185.1 24.8 %all_to_all.25 = bf16[16,2,1,12,2048]{4,0,3,2,1:T(8,128)(2,1)S(1)} all-to-all(bf16[16,2,1,12,2048]{4,0,3,2,1:T(8,128)(2,1)S(1)} %copy.204), channel_id=1, replica_groups=mesh['grp'=2,'sp_0'=16,'sp_1'=2,'tp'=4] {'sp_1'}, dimensions={1} | all-to-all | bytes 3145728 | tf_op jit(solution)/shard_map/all_to_all | solution.py:68
  211.5 72.3 %all_to_all.26 = bf16[16,2,1,12,2048]{4,1,3,2,0:T(2,128)(2,1)S(1)} all-to-all(bf16[16,2,1,12,2048]{4,1,3,2,0:T(2,128)(2,1)S(1)} %copy.205), channel_id=1, replica_groups=mesh['grp'=2,'sp_0'=16,'sp_1'=2,'tp'=4] {'sp_0'}, dimensions={0} | all-to-all | bytes 3145728 | tf_op jit(solution)/shard_map/all_to_all | solution.py:68
  283.8 2.6 copy.206
  286.4 3.7 reshape_reshape.4
  290.1 72.6 %all-gather.11.cloned.1.call-done = bf16[128,12,2048]{2,0,1:T(8,128)(2,1)} async-done(((bf16[32,12,2048]{2,0,1:T(8,128)(2,1)}), bf16[128,12,2048]{2,0,1:T(8,128)(2,1)}) %all-gather.11.cloned.1.call-update) | async-done | bytes 6291472 | tf_op jit(solution)/shard_map/all_gather | solution.py:209
  362.7 9.7 %copy.207 = bf16[128,12,2048]{2,1,0:T(8,128)(2,1)} copy(bf16[128,12,2048]{2,0,1:T(8,128)(2,1)} %all-gather.11.cloned.1.call-done) | data formatting | bytes 12582912 | tf_op jit(solution)/shard_map/all_gather | solution.py:209
  372.3 10.7 %reshape.746 = bf16[1536,2048]{1,0:T(8,128)(2,1)} reshape(bf16[128,12,2048]{2,1,0:T(8,128)(2,1)} %copy.207) | data formatting | bytes 12582912 | tf_op jit(solution)/shard_map/reshape | solution.py:212
  383.1 6.3 %convolution_minimum_fusion = f32[1536,512]{1,0:T(8,128)S(1)} fusion(bf16[1536,2048]{1,0:T(8,128)(2,1)} %reshape.746, bf16[1,2048,512]{2,1,0:T(8,128)(2,1)} %param.31), kind=kOutput, calls=%fused_computation.13 | convolution fusion | flops 3222011904 | bytes 11534336 | tf_op jit(solution)/shard_map/dot_general | solution.py:213
  389.4 5.0 fusion.7
  394.4 3.6 dot_general.53
  398.0 6.1 convert_bitcast_fusion
  404.1 73.7 %all_to_all.27 = bf16[4,1,32,12,2048]{4,2,3,1,0:T(8,128)(2,1)S(1)} all-to-all(bf16[4,1,32,12,2048]{4,2,3,1,0:T(8,128)(2,1)S(1)} %convert_bitcast_fusion), channel_id=1, replica_groups=mesh['grp'=2,'sp_0'=16,'sp_1'=2,'tp'=4] {'tp'}, dimensions={0} | all-to-all | bytes 12582912 | tf_op jit(solution)/shard_map/all_to_all | solution.py:54
  479.1 2.2 copy.211
  481.3 14.4 %all-to-all-start.4 = ((bf16[32,12,2048]{2,1,0:T(8,128)(2,1)}), bf16[32,12,2048]{2,1,0:T(8,128)(2,1)}, u32[]{:S(2)}, u32[]{:S(2)}) async-start(bf16[32,12,2048]{2,1,0:T(8,128)(2,1)} %copy.211), calls=%async_computation.4 | async-start | bytes 4194304 | tf_op jit(solution)/shard_map/all_to_all | solution.py:224
  495.9 98.6 %all-to-all-done.4 = bf16[32,12,2048]{2,1,0:T(8,128)(2,1)} async-done(((bf16[32,12,2048]{2,1,0:T(8,128)(2,1)}), bf16[32,12,2048]{2,1,0:T(8,128)(2,1)}, u32[]{:S(2)}, u32[]{:S(2)}) %all-to-all-start.4) | async-done | bytes 1572896 | tf_op jit(solution)/shard_map/all_to_all | solution.py:224
  594.4 3.6 reshape.748
  598.0 4.9 gather_fusion.1
  603.0 3.4 reshape.793
  606.4 4.9 multiply_reduce_fusion
  (159 shorter events, 48.1 us)
Async XLA Ops:
  6.5 391.5 %copy-start = (bf16[1,512,2048]{2,1,0:T(8,128)(2,1)S(1)}, bf16[1,512,2048]{2,1,0:T(8,128)(2,1)}, u32[]{:S(2)}) copy-start(bf16[1,512,2048]{2,1,0:T(8,128)(2,1)} %param.33) | copy-start | bytes 6291460
  6.6 136.0 %all-gather.9.cloned.1.call-start = ((), (), s32[]{:S(2)}) async-start(), calls=%async_computation.5 | async-start | bytes 1114112 | tf_op jit(solution)/shard_map/all_gather | solution.py:31
  19.9 2.6 copy-start.32
  22.3 26.0 %copy-start.18 = (f32[512,4]{0,1:T(4,128)S(1)}, f32[512,4]{0,1:T(4,128)}, u32[]{:S(2)}) copy-start(f32[512,4]{0,1:T(4,128)} %param.24) | copy-start | bytes 24580
  22.3 29.9 %copy-start.6 = (bf16[512,256]{1,0:T(8,128)(2,1)S(1)}, bf16[512,256]{1,0:T(8,128)(2,1)}, u32[]{:S(2)}) copy-start(bf16[512,256]{1,0:T(8,128)(2,1)} %param.21) | copy-start | bytes 786436
  22.3 30.0 %copy-start.7 = (bf16[512,256]{1,0:T(8,128)(2,1)S(1)}, bf16[512,256]{1,0:T(8,128)(2,1)}, u32[]{:S(2)}) copy-start(bf16[512,256]{1,0:T(8,128)(2,1)} %param.22) | copy-start | bytes 786436
  22.5 29.6 %copy-start.10 = (bf16[512,2,128]{2,0,1:T(8,128)(2,1)}, bf16[512,2,128]{2,0,1:T(8,128)(2,1)S(1)}, u32[]{:S(2)}) copy-start(bf16[512,2,128]{2,0,1:T(8,128)(2,1)S(1)} %fusion.41) | copy-start | bytes 786436
  47.4 2.4 copy-start.25
  53.5 2.5 copy-start.13
  54.2 82.1 %copy-start.16 = (f32[1,4,4,128]{3,1,2,0:T(4,128)S(1)}, f32[1,4,4,128]{3,1,2,0:T(4,128)}, u32[]{:S(2)}) copy-start(f32[1,4,4,128]{3,1,2,0:T(4,128)} %copy-done.15) | copy-start | bytes 24580
  56.0 4.3 copy-start.11
  56.0 4.4 copy-start.12
  60.2 76.1 %copy-start.28 = (f32[4]{0:T(128)}, f32[4]{0:T(128)S(1)}, u32[]{:S(2)}) copy-start(f32[4]{0:T(128)S(1)} %get-tuple-element.66) | copy-start | bytes 52
  60.2 76.0 %copy-start.29 = (f32[4]{0:T(128)}, f32[4]{0:T(128)S(1)}, u32[]{:S(2)}) copy-start(f32[4]{0:T(128)S(1)} %get-tuple-element.67) | copy-start | bytes 52
  136.3 4.1 copy-start.14
  140.4 2.0 copy-start.24
  140.4 2.2 copy-start.20
  140.4 2.2 copy-start.26
  142.4 3.2 copy-start.8
  142.4 3.2 copy-start.9
  142.5 3.2 copy-start.22
  148.3 2.1 copy-start.5
  152.4 4.8 copy-start.19
  152.4 20.0 %all-to-all-start = ((bf16[4,128,2048]{2,1,0:T(8,128)(2,1)}), bf16[4,128,2048]{2,1,0:T(8,128)(2,1)}, u32[]{:S(2)}, u32[]{:S(2)}) async-start(bf16[4,128,2048]{2,1,0:T(8,128)(2,1)} %bitcast.468), calls=%async_computation | async-start | bytes 4194304 | tf_op jit(solution)/shard_map/all_to_all | solution.py:54
  157.1 17.5 %copy-start.4 = (bf16[128,2048]{1,0:T(8,128)(2,1)S(1)}, bf16[128,2048]{1,0:T(8,128)(2,1)}, u32[]{:S(2)}) copy-start(bf16[128,2048]{1,0:T(8,128)(2,1)} %param.25) | copy-start | bytes 1572868
  157.1 205.6 %all-gather.11.cloned.1.call-start = ((), (), s32[]{:S(2)}) async-start(), calls=%async_computation.6 | async-start | bytes 7864320 | tf_op jit(solution)/shard_map/all_gather | solution.py:209
  160.2 15.3 %copy-start.17 = (f32[2048]{0:T(1024)S(1)}, f32[2048]{0:T(1024)}, u32[]{:S(2)}) copy-start(f32[2048]{0:T(1024)} %param.28) | copy-start | bytes 24580
  383.1 6.3 %copy-start.3 = (bf16[1536,2048]{1,0:T(8,128)(2,1)S(1)}, bf16[1536,2048]{1,0:T(8,128)(2,1)}, u32[]{:S(2)}) copy-start(bf16[1536,2048]{1,0:T(8,128)(2,1)} %reshape.746) | copy-start | bytes 18874372
  383.1 6.3 %copy-start.31 = (bf16[1,2048,512]{2,1,0:T(8,128)(2,1)S(1)}, bf16[1,2048,512]{2,1,0:T(8,128)(2,1)}, u32[]{:S(2)}) copy-start(bf16[1,2048,512]{2,1,0:T(8,128)(2,1)} %param.32) | copy-start | bytes 6291460
  481.3 14.4 %copy-start.30 = (f32[128,2]{0,1:T(2,128)S(1)}, f32[128,2]{0,1:T(2,128)}, u32[]{:S(2)}) copy-start(f32[128,2]{0,1:T(2,128)} %param.30) | copy-start | bytes 3076
  481.3 113.1 %all-to-all-start.4 = ((bf16[32,12,2048]{2,1,0:T(8,128)(2,1)}), bf16[32,12,2048]{2,1,0:T(8,128)(2,1)}, u32[]{:S(2)}, u32[]{:S(2)}) async-start(bf16[32,12,2048]{2,1,0:T(8,128)(2,1)} %copy.211), calls=%async_computation.4 | async-start | bytes 4194304 | tf_op jit(solution)/shard_map/all_to_all | solution.py:224
  606.4 4.9 copy-start.2
  (5 other events, 4.4 us)
Sparse Core Ops, SparseCore 0:
  48.3 54.4 all-gather.8
  290.2 72.4 all-gather.10
where the time goes:
time: 626 us; the launch traced here: 619 us
  blocking collectives  273 us (44%)
  waiting for transfers between devices  184 us (29%)
  local copies, waits for them, and re-layouts  72.1 us (12%)
  matrix products  33.7 us (5%)
  other arithmetic  24.1 us (4%)
  starting transfers between devices  19.1 us (3%)
  between operations  14.3 us (2%)
    all_gather x7, blocking collectives, prefix_by_axis(): lax.all_gather(part.astype(kind), axis)  102 us
    all_to_all x1, waiting for transfers between devices, body(): lax.all_to_all(expert_output, SP, split_axis=0, concat_axis=0, tiled=True)  98.6 us
    all_to_all x2, blocking collectives, turned_blocks(): filled = lax.all_to_all(filled, axes[k], k, k, tiled=True)  97.1 us
    all_to_all x1, blocking collectives, sent_and_summed(): lax.all_to_all(pieces, axis, split_axis=0, concat_axis=0, tiled=True)  73.7 us
    all_gather x1, waiting for transfers between devices, body(): lax.all_gather(core_and_chips(send_slots, ('sp_0', 'sp_1'), (1, 0), 0, 0)...  72.6 us
    all_to_all x1, starting transfers between devices, body(): lax.all_to_all(expert_output, SP, split_axis=0, concat_axis=0, tiled=True)  14.4 us
  transfers between devices with their start and end apart: 4, of which 3 were waited for; matrix products, arithmetic and copies ran while one was open for 3% of the time, Pallas kernels for 0%

commit v1 on v0

--- a/solution.py
+++ b/solution.py
@@ -206,9 +206,17 @@
     gate_shard = expert_gate[0]
     up_shard = expert_up[0]
     down_shard = expert_down[0]
-    gathered = lax.all_gather(
-        core_and_chips(send_slots, ("sp_0", "sp_1"), (1, 0), 0, 0), "tp", axis=0, tiled=True
-    )
+    shard = core_and_chips(send_slots, ("sp_0", "sp_1"), (1, 0), 0, 0)
+    ways = lax.axis_size("tp")
+    up = [(d, (d + 1) % ways) for d in range(ways)]
+    down = [(d, (d - 1) % ways) for d in range(ways)]
+    earlier_2, later_2 = ([shard], [shard])
+    for _ in range(ways // 2):
+        earlier_2.append(lax.ppermute(earlier_2[-1], "tp", up))
+    for _ in range((ways - 1) // 2):
+        later_2.append(lax.ppermute(later_2[-1], "tp", down))
+    line = jnp.concatenate([*earlier_2[::-1], *later_2[1:]], axis=0)
+    gathered = jnp.roll(line, (lax.axis_index("tp") - ways // 2) * shard.shape[0], axis=0)
     flat_rows = gathered.reshape(-1, model_width)
     gate_pre = jnp.dot(flat_rows, gate_shard, preferred_element_type=jnp.float32)
     up_pre = jnp.dot(flat_rows, up_shard, preferred_element_type=jnp.float32)

time: 626 us -> 649 us (1.037)
  starting transfers between devices: 19.1 us -> 40.8 us
  local copies, waits for them, and re-layouts: 72.1 us -> 93.7 us
  waiting for transfers between devices: 184 us -> 171 us
  blocking collectives: 273 us -> 264 us
    all_gather x1 -> x0, waiting for transfers between devices: 72.6 us -> none  [body(): lax.all_gather(core_and_chips(send_slots, ('sp_0', 'sp_1'), (1, 0), 0, 0)...]
    ppermute x0 -> x3, waiting for transfers between devices: none -> 60.1 us  [the longest x2 60.1 us: body(): earlier_2.append(lax.ppermute(earlier_2[-1], 'tp', up))]
    all_to_all x1, starting transfers between devices: 14.4 us -> 33.2 us  [body(): lax.all_to_all(expert_output, SP, split_axis=0, concat_axis=0, tiled=True)]
    unnamed x77 -> x86, local copies, waits for them, and re-layouts: 10.4 us -> 26.9 us
    dynamic_slice x0 -> x2, local copies, waits for them, and re-layouts: none -> 10.4 us  [body(): jnp.roll(line, (lax.axis_index('tp') - ways // 2) * shard.shape[0], axis=0)]
    all_gather x1 -> x0, local copies, waits for them, and re-layouts: 9.65 us -> none  [body(): lax.all_gather(core_and_chips(send_slots, ('sp_0', 'sp_1'), (1, 0), 0, 0)...]
    all_to_all x1, blocking collectives: 73.7 us -> 65.3 us  [sent_and_summed(): lax.all_to_all(pieces, axis, split_axis=0, concat_axis=0, tiled=True)]
  transfers between devices with their start and end apart: 4 -> 6, of which waited for: 3 -> 4; matrix products, arithmetic and copies ran while one was open for 3% -> 4% of each run, Pallas kernels for 0% -> 0%
where the time goes in v1:
time: 649 us; the launch traced here: 642 us
  blocking collectives  264 us (41%)
  waiting for transfers between devices  171 us (26%)
  local copies, waits for them, and re-layouts  93.7 us (14%)
  starting transfers between devices  40.8 us (6%)
  matrix products  33.7 us (5%)
  other arithmetic  24.5 us (4%)
  between operations  14.3 us (2%)
    all_gather x7, blocking collectives, prefix_by_axis(): lax.all_gather(part.astype(kind), axis)  101 us
    all_to_all x1, waiting for transfers between devices, body(): lax.all_to_all(expert_output, SP, split_axis=0, concat_axis=0, tiled=True)  98.6 us
    all_to_all x2, blocking collectives, turned_blocks(): filled = lax.all_to_all(filled, axes[k], k, k, tiled=True)  97.5 us
    all_to_all x1, blocking collectives, sent_and_summed(): lax.all_to_all(pieces, axis, split_axis=0, concat_axis=0, tiled=True)  65.3 us
    ppermute x2, waiting for transfers between devices, body(): earlier_2.append(lax.ppermute(earlier_2[-1], 'tp', up))  60.1 us
    all_to_all x1, starting transfers between devices, body(): lax.all_to_all(expert_output, SP, split_axis=0, concat_axis=0, tiled=True)  33.2 us
    unnamed x86, local copies, waits for them, and re-layouts  26.9 us
  transfers between devices with their start and end apart: 6, of which 4 were waited for; matrix products, arithmetic and copies ran while one was open for 4% of the time, Pallas kernels for 0%

profile of v1, /device:TPU:33, one launch (start us, length us, event | category | flops | bytes accessed | tf_op | source)
XLA Modules:
  0.0 642.0 jit_solution(1093117172707395520)
XLA Ops:
  23.6 22.0 %all-gather = bf16[4,128,128]{2,1,0:T(8,128)(2,1)S(1)} all-gather(bf16[2,128,128]{2,1,0:T(8,128)(2,1)S(1)} %convolution_convert_fusion.1), channel_id=2, replica_groups=mesh['grp'=2,'sp_0'=16,'sp_1'=2,'tp'=4] {'sp_1'}, dimensions={0}, use_global_device_ids=true | all-gather | bytes 196608 | tf_op jit(solution)/shard_map/all_gather | solution.py:31
  62.4 32.0 %all_gather.45 = bf16[16,4,64,64]{3,2,1,0:T(8,128)(2,1)S(1)} all-gather(bf16[1,4,64,64]{3,2,1,0:T(8,128)(2,1)S(1)} %fusion.70), channel_id=1, replica_groups=mesh['grp'=2,'sp_0'=16,'sp_1'=2,'tp'=4] {'sp_0'}, dimensions={0}, use_global_device_ids=true | all-gather | bytes 557056 | tf_op jit(solution)/shard_map/all_gather | solution.py:31
  94.4 20.6 %all-gather.5 = bf16[16,1,4]{2,1,0:T(2,128)(2,1)S(1)} all-gather(bf16[1,1,4]{2,1,0:T(2,128)(2,1)S(1)} %get-tuple-element.65), channel_id=1, replica_groups=mesh['grp'=2,'sp_0'=16,'sp_1'=2,'tp'=4] {'sp_0'}, dimensions={0}, use_global_device_ids=true | all-gather | bytes 136 | tf_op jit(solution)/shard_map/all_gather | solution.py:31
  115.7 20.9 %all-gather.3 = bf16[16,1,2]{2,1,0:T(2,128)(2,1)S(1)} all-gather(bf16[1,1,2]{2,1,0:T(2,128)(2,1)} %get-tuple-element.68), channel_id=1, replica_groups=mesh['grp'=2,'sp_0'=16,'sp_1'=2,'tp'=4] {'sp_0'}, dimensions={0}, use_global_device_ids=true | all-gather | bytes 68 | tf_op jit(solution)/shard_map/all_gather | solution.py:31
  138.0 4.1 fusion.31
  144.2 3.1 fusion.34
  154.1 4.7 all-to-all-start
  161.8 12.3 %all-to-all-done = bf16[4,128,2048]{2,1,0:T(8,128)(2,1)} async-done(((bf16[4,128,2048]{2,1,0:T(8,128)(2,1)}), bf16[4,128,2048]{2,1,0:T(8,128)(2,1)}, u32[]{:S(2)}, u32[]{:S(2)}) %all-to-all-start) | async-done | bytes 2097184 | tf_op jit(solution)/shard_map/all_to_all | solution.py:54
  177.6 3.1 gather_fusion
  180.7 3.6 reshape_reshape_reshape.3
  186.7 24.4 %all_to_all.25 = bf16[16,2,1,12,2048]{4,0,3,2,1:T(8,128)(2,1)S(1)} all-to-all(bf16[16,2,1,12,2048]{4,0,3,2,1:T(8,128)(2,1)S(1)} %copy.204), channel_id=1, replica_groups=mesh['grp'=2,'sp_0'=16,'sp_1'=2,'tp'=4] {'sp_1'}, dimensions={1} | all-to-all | bytes 3145728 | tf_op jit(solution)/shard_map/all_to_all | solution.py:68
  212.8 73.1 %all_to_all.26 = bf16[16,2,1,12,2048]{4,1,3,2,0:T(2,128)(2,1)S(1)} all-to-all(bf16[16,2,1,12,2048]{4,1,3,2,0:T(2,128)(2,1)S(1)} %copy.205), channel_id=1, replica_groups=mesh['grp'=2,'sp_0'=16,'sp_1'=2,'tp'=4] {'sp_0'}, dimensions={0} | all-to-all | bytes 3145728 | tf_op jit(solution)/shard_map/all_to_all | solution.py:68
  288.4 3.7 reshape_reshape.4
  292.4 29.9 %collective-permute-done = bf16[32,12,2048]{2,0,1:T(8,128)(2,1)} collective-permute-done((bf16[32,12,2048]{2,0,1:T(8,128)(2,1)}, bf16[32,12,2048]{2,0,1:T(8,128)(2,1)}, u32[]{:S(2)}, u32[]{:S(2)}) %collective-permute-start) | collective-permute-done | bytes 1572896 | tf_op jit(solution)/shard_map/ppermute | solution.py:215
  325.0 30.2 %collective-permute-done.1 = bf16[32,12,2048]{2,0,1:T(8,128)(2,1)} collective-permute-done((bf16[32,12,2048]{2,0,1:T(8,128)(2,1)}, bf16[32,12,2048]{2,0,1:T(8,128)(2,1)}, u32[]{:S(2)}, u32[]{:S(2)}) %collective-permute-start.1) | collective-permute-done | bytes 1572896 | tf_op jit(solution)/shard_map/ppermute | solution.py:215
  361.9 2.8 constant_dynamic-update-slice_fusion.4
  367.3 2.8 constant_dynamic-update-slice_fusion.2
  371.4 2.8 constant_dynamic-update-slice_fusion
  374.2 3.6 constant_dynamic-slice_fusion
  377.7 6.9 %copy.207 = bf16[128,12,2048]{2,1,0:T(8,128)(2,1)} copy(bf16[128,12,2048]{2,0,1:T(8,128)(2,1)S(1)} %constant_dynamic-slice_fusion) | data formatting | bytes 12582912 | tf_op jit(solution)/shard_map/jit(_roll_dynamic)/dynamic_slice | solution.py:219
  384.6 10.7 %reshape.746 = bf16[1536,2048]{1,0:T(8,128)(2,1)} reshape(bf16[128,12,2048]{2,1,0:T(8,128)(2,1)} %copy.207) | data formatting | bytes 12582912 | tf_op jit(solution)/shard_map/reshape | solution.py:220
  395.3 6.3 convolution_minimum_fusion
  401.6 5.0 fusion.7
  406.6 3.6 dot_general.53
  410.2 6.1 convert_bitcast_fusion
  416.4 65.3 %all_to_all.27 = bf16[4,1,32,12,2048]{4,2,3,1,0:T(8,128)(2,1)S(1)} all-to-all(bf16[4,1,32,12,2048]{4,2,3,1,0:T(8,128)(2,1)S(1)} %convert_bitcast_fusion), channel_id=1, replica_groups=mesh['grp'=2,'sp_0'=16,'sp_1'=2,'tp'=4] {'tp'}, dimensions={0} | all-to-all | bytes 12582912 | tf_op jit(solution)/shard_map/all_to_all | solution.py:54
  485.1 33.2 %all-to-all-start.4 = ((bf16[32,12,2048]{2,1,0:T(8,128)(2,1)}), bf16[32,12,2048]{2,1,0:T(8,128)(2,1)}, u32[]{:S(2)}, u32[]{:S(2)}) async-start(bf16[32,12,2048]{2,1,0:T(8,128)(2,1)} %copy.211), calls=%async_computation.4 | async-start | bytes 4194304 | tf_op jit(solution)/shard_map/all_to_all | solution.py:232
  518.5 98.6 %all-to-all-done.4 = bf16[32,12,2048]{2,1,0:T(8,128)(2,1)} async-done(((bf16[32,12,2048]{2,1,0:T(8,128)(2,1)}), bf16[32,12,2048]{2,1,0:T(8,128)(2,1)}, u32[]{:S(2)}, u32[]{:S(2)}) %all-to-all-start.4) | async-done | bytes 1572896 | tf_op jit(solution)/shard_map/all_to_all | solution.py:232
  617.1 3.6 reshape.748
  620.7 4.9 gather_fusion.1
  625.6 3.5 reshape.793
  629.1 4.9 multiply_reduce_fusion
  (173 shorter events, 75.7 us)
Async XLA Ops:
  6.5 403.7 %copy-start = (bf16[1,512,2048]{2,1,0:T(8,128)(2,1)S(1)}, bf16[1,512,2048]{2,1,0:T(8,128)(2,1)}, u32[]{:S(2)}) copy-start(bf16[1,512,2048]{2,1,0:T(8,128)(2,1)} %param.33) | copy-start | bytes 6291460
  6.6 137.7 %all-gather.8.cloned.1.call-start = ((), (), s32[]{:S(2)}) async-start(), calls=%async_computation.5 | async-start | bytes 1114112 | tf_op jit(solution)/shard_map/all_gather | solution.py:31
  18.3 4.8 copy-start.32
  19.9 29.0 %copy-start.19 = (f32[512,4]{0,1:T(4,128)S(1)}, f32[512,4]{0,1:T(4,128)}, u32[]{:S(2)}) copy-start(f32[512,4]{0,1:T(4,128)} %param.24) | copy-start | bytes 24580
  22.2 31.8 %copy-start.8 = (bf16[512,256]{1,0:T(8,128)(2,1)S(1)}, bf16[512,256]{1,0:T(8,128)(2,1)}, u32[]{:S(2)}) copy-start(bf16[512,256]{1,0:T(8,128)(2,1)} %param.22) | copy-start | bytes 786436
  48.1 2.4 copy-start.26
  54.0 84.0 %copy-start.17 = (f32[1,4,4,128]{3,1,2,0:T(4,128)S(1)}, f32[1,4,4,128]{3,1,2,0:T(4,128)}, u32[]{:S(2)}) copy-start(f32[1,4,4,128]{3,1,2,0:T(4,128)} %copy-done.16) | copy-start | bytes 24580
  55.2 3.0 copy-start.14
  55.3 5.2 copy-start.33
  58.2 4.0 copy-start.12
  58.2 4.1 copy-start.13
  62.3 75.7 %copy-start.28 = (f32[4]{0:T(128)}, f32[4]{0:T(128)S(1)}, u32[]{:S(2)}) copy-start(f32[4]{0:T(128)S(1)} %get-tuple-element.66) | copy-start | bytes 52
  62.3 75.7 %copy-start.29 = (f32[4]{0:T(128)}, f32[4]{0:T(128)S(1)}, u32[]{:S(2)}) copy-start(f32[4]{0:T(128)S(1)} %get-tuple-element.67) | copy-start | bytes 52
  137.9 4.1 copy-start.15
  142.1 2.2 copy-start.21
  143.9 3.4 copy-start.9
  143.9 3.4 copy-start.10
  144.0 3.4 copy-start.23
  154.1 4.7 copy-start.20
  154.1 22.1 %copy-start.5 = (bf16[128,2048]{1,0:T(8,128)(2,1)S(1)}, bf16[128,2048]{1,0:T(8,128)(2,1)}, u32[]{:S(2)}) copy-start(bf16[128,2048]{1,0:T(8,128)(2,1)} %param.25) | copy-start | bytes 1572868
  154.1 20.0 %all-to-all-start = ((bf16[4,128,2048]{2,1,0:T(8,128)(2,1)}), bf16[4,128,2048]{2,1,0:T(8,128)(2,1)}, u32[]{:S(2)}, u32[]{:S(2)}) async-start(bf16[4,128,2048]{2,1,0:T(8,128)(2,1)} %bitcast.468), calls=%async_computation | async-start | bytes 4194304 | tf_op jit(solution)/shard_map/all_to_all | solution.py:54
  158.8 18.5 %copy-start.18 = (f32[2048]{0:T(1024)S(1)}, f32[2048]{0:T(1024)}, u32[]{:S(2)}) copy-start(f32[2048]{0:T(1024)} %param.28) | copy-start | bytes 24580
  292.1 30.2 %collective-permute-start = (bf16[32,12,2048]{2,0,1:T(8,128)(2,1)}, bf16[32,12,2048]{2,0,1:T(8,128)(2,1)}, u32[]{:S(2)}, u32[]{:S(2)}) collective-permute-start(bf16[32,12,2048]{2,0,1:T(8,128)(2,1)} %reshape_reshape.4), channel_id=1, source_target_pairs={{0,1},{1,2},{2,3},{3,0},{4,5},{5,6},{6,7},{7,4},{8,9},{9,10},{10,1... | collective-permute-start | bytes 4718600 | tf_op jit(solution)/shard_map/ppermute | solution.py:215
  322.3 32.9 %collective-permute-start.1 = (bf16[32,12,2048]{2,0,1:T(8,128)(2,1)}, bf16[32,12,2048]{2,0,1:T(8,128)(2,1)}, u32[]{:S(2)}, u32[]{:S(2)}) collective-permute-start(bf16[32,12,2048]{2,0,1:T(8,128)(2,1)} %collective-permute-done), channel_id=1, source_target_pairs={{0,1},{1,2},{2,3},{3,0},{4,5},{5,6},{6,7},{7,4},{8,9},{9,10},{10,1... | collective-permute-start | bytes 4718600 | tf_op jit(solution)/shard_map/ppermute | solution.py:215
  322.3 39.6 %collective-permute-start.2 = (bf16[32,12,2048]{2,0,1:T(8,128)(2,1)}, bf16[32,12,2048]{2,0,1:T(8,128)(2,1)}, u32[]{:S(2)}, u32[]{:S(2)}) collective-permute-start(bf16[32,12,2048]{2,0,1:T(8,128)(2,1)} %reshape_reshape.4), channel_id=1, source_target_pairs={{0,3},{1,0},{2,1},{3,2},{4,7},{5,4},{6,5},{7,6},{8,11},{9,8},{10,9... | collective-permute-start | bytes 4718600 | tf_op jit(solution)/shard_map/ppermute | solution.py:217
  325.0 35.6 %copy-start.3 = (bf16[32,12,2048]{2,0,1:T(8,128)(2,1)S(1)}, bf16[32,12,2048]{2,0,1:T(8,128)(2,1)}, u32[]{:S(2)}) copy-start(bf16[32,12,2048]{2,0,1:T(8,128)(2,1)} %reshape_reshape.4) | copy-start | bytes 4718596
  395.3 6.3 copy-start.4
  395.3 6.3 copy-start.31
  482.9 35.4 %copy-start.30 = (f32[128,2]{0,1:T(2,128)S(1)}, f32[128,2]{0,1:T(2,128)}, u32[]{:S(2)}) copy-start(f32[128,2]{0,1:T(2,128)} %param.30) | copy-start | bytes 3076
  485.1 131.9 %all-to-all-start.4 = ((bf16[32,12,2048]{2,1,0:T(8,128)(2,1)}), bf16[32,12,2048]{2,1,0:T(8,128)(2,1)}, u32[]{:S(2)}, u32[]{:S(2)}) async-start(bf16[32,12,2048]{2,1,0:T(8,128)(2,1)} %copy.211), calls=%async_computation.4 | async-start | bytes 4194304 | tf_op jit(solution)/shard_map/all_to_all | solution.py:232
  625.6 8.4 %copy-start.2 = (f32[128,2048]{1,0:T(8,128)S(1)}, f32[128,2048]{1,0:T(8,128)}, u32[]{:S(2)}) copy-start(f32[128,2048]{1,0:T(8,128)} %copy-done.1) | copy-start | bytes 3145732
  629.1 4.9 copy-start.6
  (8 other events, 9.3 us)
Sparse Core Ops, SparseCore 0:
  49.0 54.4 all-gather.7
